TPU v7x, 32 devices: a whole 2x2x4 slice. The times are simulated.
32 devices in a mesh: sp: 16 (over z, y, x), tp: 2 (over core).
Axes of the slice: x: 2, y: 2, z: 4, core: 2. Of those that a mesh axis runs over, the one named last changes fastest.
Arguments:
- queries: bfloat16 [4096, 1024], P('sp', 'tp'), may hold values from -100 to 100
- keys: bfloat16 [256, 4096], P('tp', 'sp'), may hold values from -5 to 5
- values: bfloat16 [256, 4096], P('tp', 'sp'), may hold values from -4.5 to 4.5
- gate_cache: float32 [8, 4096], P('tp', 'sp'), as said below
- documents: int32 [4096], P('sp'), may hold values from 0 to 2, never falling along the last dimension, each value on 1 to 2560 neighbouring positions
- residual: bfloat16 [4096, 2048], P(('sp', 'tp')), may hold values from -3 to 3
- out_weight: bfloat16 [1024, 2048], replicated, may hold values from -2 to 2
- mix_gain: bfloat16 [2048], replicated, may hold values from 0.099609375 to 1.8984375
- routes: int32 [4096, 4], P(('sp', 'tp')), may hold values from 0 to 31, all different within a row; in each aligned block of 128 rows (0 to 127, 128 to 255, ...) at most 32 rows name the same one
- route_weight: float32 [4096, 4], P(('sp', 'tp')), may hold values from 0.25 to 1
- expert_gate: bfloat16 [32, 2048, 512], P(('sp', 'tp')), may hold values from -0.125 to 0.125
- expert_up: bfloat16 [32, 2048, 512], P(('sp', 'tp')), may hold values from -0.125 to 0.125
- expert_down: bfloat16 [32, 512, 2048], P(('sp', 'tp')), may hold values from -0.25 to 0.25
- shared_gate: bfloat16 [2048, 512], replicated, may hold values from -0.125 to 0.125
- shared_up: bfloat16 [2048, 512], replicated, may hold values from -0.125 to 0.125
- shared_down: bfloat16 [512, 2048], replicated, may hold values from -0.25 to 0.25
- ffn_gain: bfloat16 [2048], replicated, may hold values from 0.099609375 to 1.8984375
Outputs:
- result: bfloat16 [4096, 2048], P(('sp', 'tp'))
Inputs may be any that keep to these rules, and one draw needn't show every extreme that they name: `gate_cache`: entry (h, j) is the sum of head h's log forget gates over positions 0 to j. `documents`: never falls along the positions; no document has more than 2560 positions. `routes`: each row names 4 different experts; in the rows of one device (aligned blocks of 128 rows) no expert is named more than 32 times, a bound that some block reaches.
All inputs are finite; a program needn't handle non-finite values.
Results may differ from a plain program's by a relative error of at most 0.013.
Values may be sent and summed in bfloat16 or wider, within the bound.
A program may use at most 256 MiB of HBM per device.

v0:
```python
import jax
import jax.numpy as jnp
from jax import lax
from jax.sharding import PartitionSpec as P

HD = 128
residual_scale = 2.0**0.25
norm_epsilon = 1e-05
masked_score = -1e30


def normalize(summed, gain_vector):
    row_mean = jnp.mean(summed, axis=-1, keepdims=True)
    centred = summed - row_mean
    spread = jnp.mean(centred * centred, axis=-1, keepdims=True)
    return (centred * lax.rsqrt(spread + norm_epsilon) * gain_vector.astype(jnp.float32)).astype(
        jnp.bfloat16
    )


def expert_block(arrived, expert_gate, expert_up, expert_down):
    own_count = expert_gate.shape[0]
    grouped = arrived.reshape(-1, own_count, arrived.shape[1], arrived.shape[2])
    gate_part = jnp.einsum(
        "nemd,edf->nemf", grouped, expert_gate, preferred_element_type=jnp.float32
    )
    up_part = jnp.einsum("nemd,edf->nemf", grouped, expert_up, preferred_element_type=jnp.float32)
    hidden = (jax.nn.silu(gate_part) * up_part).astype(jnp.bfloat16)
    produced = jnp.einsum("nemf,efd->nemd", hidden, expert_down, preferred_element_type=jnp.float32)
    return produced.astype(jnp.bfloat16).reshape(arrived.shape)


def local(
    queries,
    keys,
    values,
    gate_cache,
    documents,
    residual,
    out_weight,
    mix_gain,
    routes,
    route_weight,
    expert_gate,
    expert_up,
    expert_down,
    shared_gate,
    shared_up,
    shared_down,
    ffn_gain,
):
    tok_rows = queries.shape[0]
    local_heads = gate_cache.shape[0]
    kv_local = keys.shape[0] // HD
    group_size = local_heads // kv_local
    score_scale = HD ** (-0.5)
    seq_start = lax.axis_index("sp") * tok_rows
    query_pos = seq_start + jnp.arange(tok_rows, dtype=jnp.int32)
    query_last = seq_start + tok_rows - 1
    query_cum = jnp.transpose(gate_cache).reshape(tok_rows, kv_local, group_size)
    grouped_q = queries.reshape(tok_rows, kv_local, group_size, HD)
    all_cache, all_docs = (
        lax.all_gather(gate_cache, "sp", axis=1, tiled=True),
        lax.all_gather(documents.reshape(1, tok_rows), "sp", axis=1, tiled=True),
    )
    doc_line = all_docs[0]
    initial = (
        jnp.full((tok_rows, kv_local, group_size), masked_score, jnp.float32),
        jnp.zeros((tok_rows, kv_local, group_size), jnp.float32),
        jnp.zeros((tok_rows, kv_local, group_size, HD), jnp.float32),
    )
    key_piece = lax.all_gather(keys, "sp", axis=1, tiled=True)
    value_piece = lax.all_gather(values, "sp", axis=1, tiled=True)
    width_keys = key_piece.shape[1]
    key_cum = all_cache.reshape(kv_local, group_size, width_keys)

    def update(state):
        running_max, running_sum, numerator = state
        key_block = key_piece.reshape(kv_local, HD, width_keys)
        value_block = value_piece.reshape(kv_local, HD, width_keys)
        scores = (
            jnp.einsum("qagd,adk->qagk", grouped_q, key_block, preferred_element_type=jnp.float32)
            * score_scale
        )
        scores = scores + query_cum[..., None] - key_cum[None]
        key_pos = jnp.arange(width_keys, dtype=jnp.int32)
        allowed = (key_pos[None, :] <= query_pos[:, None]) & (
            doc_line[None, :] == documents[:, None]
        )
        allowed = allowed[:, None, None, :]
        scores = jnp.where(allowed, scores, masked_score)
        new_max = jnp.maximum(running_max, jnp.max(scores, axis=-1))
        weights = jnp.where(allowed, jnp.exp(scores - new_max[..., None]), 0.0)
        new_sum = jnp.sum(weights, axis=-1)
        added = jnp.einsum(
            "qagk,adk->qagd",
            weights.astype(jnp.bfloat16),
            value_block,
            preferred_element_type=jnp.float32,
        )
        return (new_max, new_sum, added)

    active = (jnp.int32(0) <= query_last) & (doc_line[width_keys - 1] >= documents[0])
    running_max, running_sum, numerator = lax.cond(active, update, lambda state: state, initial)
    attended = (
        (numerator / running_sum[..., None])
        .astype(jnp.bfloat16)
        .reshape(tok_rows, local_heads * HD)
    )
    token_heads = lax.all_to_all(attended, "tp", split_axis=0, concat_axis=1, tiled=True)
    mixed = jnp.dot(token_heads, out_weight, preferred_element_type=jnp.float32)
    mixed = lax.optimization_barrier(mixed.astype(jnp.bfloat16)).astype(jnp.float32)
    settled = normalize(residual_scale * residual.astype(jnp.float32) + mixed, mix_gain)
    row_count = settled.shape[0]
    width_model = settled.shape[1]
    top_count = routes.shape[1]
    expert_total = lax.axis_size(("sp", "tp")) * expert_gate.shape[0]
    capacity = row_count * lax.axis_size("tp") * top_count // expert_total
    chosen_experts = routes.reshape(-1)
    matches = (
        chosen_experts[:, None] == jnp.arange(expert_total, dtype=jnp.int32)[None, :]
    ).astype(jnp.int32)
    ranks = jnp.sum(jnp.cumsum(matches, axis=0) * matches, axis=1) - 1
    slots = chosen_experts * capacity + ranks
    placing = slots[None, :] == jnp.arange(expert_total * capacity, dtype=jnp.int32)[:, None]
    placing = jnp.any(
        placing.reshape(expert_total * capacity, row_count, top_count), axis=2
    ).astype(jnp.bfloat16)
    outgoing = jnp.dot(placing, settled, preferred_element_type=jnp.float32).astype(jnp.bfloat16)
    outgoing = outgoing.reshape(expert_total, capacity, width_model)
    finished = expert_block(
        lax.all_to_all(outgoing, ("sp", "tp"), split_axis=0, concat_axis=0, tiled=True),
        expert_gate,
        expert_up,
        expert_down,
    )
    returned = lax.all_to_all(finished, ("sp", "tp"), split_axis=0, concat_axis=0, tiled=True)
    returned = returned.reshape(expert_total * capacity, width_model)
    picked_rows = jnp.take(returned, slots, axis=0).reshape(row_count, top_count, width_model)
    routed = jnp.einsum("rkd,rk->rd", picked_rows.astype(jnp.float32), route_weight)
    shared_gate_part = jnp.dot(settled, shared_gate, preferred_element_type=jnp.float32)
    shared_up_part = jnp.dot(settled, shared_up, preferred_element_type=jnp.float32)
    shared_hidden = (jax.nn.silu(shared_gate_part) * shared_up_part).astype(jnp.bfloat16)
    shared = jnp.dot(shared_hidden, shared_down, preferred_element_type=jnp.float32)
    return normalize(residual_scale * settled.astype(jnp.float32) + routed + shared, ffn_gain)


def solution(mesh):
    placed = (
        P("sp", "tp"),
        P("tp", "sp"),
        P("tp", "sp"),
        P("tp", "sp"),
        P("sp"),
        P(("sp", "tp"), None),
        P(),
        P(),
        P(("sp", "tp"), None),
        P(("sp", "tp"), None),
        P(("sp", "tp"), None, None),
        P(("sp", "tp"), None, None),
        P(("sp", "tp"), None, None),
        P(),
        P(),
        P(),
        P(),
    )
    return jax.shard_map(
        local, mesh=mesh, in_specs=placed, out_specs=P(("sp", "tp"), None), check_vma=False
    )
```

profile of v0, /device:TPU:0, one launch (start us, length us, event | category | flops | bytes accessed | tf_op | source)
XLA Modules:
  0.0 393.6 jit_solution(2535516395564024456)
XLA Ops:
  6.5 1.7 copy.56
  8.3 0.7 all-gather.7.cloned.1.call-update
  9.0 0.8 copy.59
  9.8 0.1 eq.59
  9.9 0.1 reshape.234
  10.1 1.2 slice.14
  11.3 42.7 %all-gather.1 = s32[16,1,256]{2,1,0:T(1,128)S(1)} all-gather(s32[1,1,256]{2,1,0:T(1,128)} %bitcast.172), channel_id=2, replica_groups=mesh['sp'=16,'tp'=2] {'sp'}, dimensions={0}, use_global_device_ids=true | all-gather | bytes 17408 | tf_op jit(solution)/shard_map/all_gather | solution.py:64
  54.0 0.6 slice.19
  55.8 0.7 convert_element_type.60
  56.5 1.2 reduce-window.6
  57.7 0.2 slice_reduce_fusion
  58.0 0.1 fusion.50
  58.1 0.1 sub.47
  58.3 36.1 %all_gather.14 = f32[4,4096]{1,0:T(4,128)S(1)} all-gather(f32[4,256]{1,0:T(4,128)} %param.22), channel_id=1, replica_groups=mesh['sp'=16,'tp'=2] {'sp'}, dimensions={1}, use_global_device_ids=true | all-gather | bytes 69632 | tf_op jit(solution)/shard_map/all_gather | solution.py:63
  94.4 0.7 compare_and_fusion
  95.1 0.4 fusion.31
  95.4 29.3 %all-gather.7.cloned.1.call-done = bf16[128,4096]{1,0:T(8,128)(2,1)} async-done(((bf16[128,256]{1,0:T(8,128)(2,1)}), bf16[128,4096]{1,0:T(8,128)(2,1)}) %all-gather.7.cloned.1.call-update) | async-done | bytes 1048592 | tf_op jit(solution)/shard_map/all_gather | solution.py:73
  124.7 20.7 %conditional.1 = (f32[256,1,4]{0,2,1:T(4,128)S(1)}, f32[256,1,4,128]{3,0,2,1:T(8,128)S(1)}) conditional(s32[]{:T(128)} %convert_element_type.56, () %tuple.13, (s32[]{:T(128)}, s32[256]{0:T(256)S(1)}, s32[1,4096]{1,0:T(1,128)S(1)}, s32[256]{0:T(256)}, bf16[256,512]{1,0:T(8,128)(2,1)}, /*index=5*/bf16[128,4096]{0,1:T(8,128)(2,1)}, f32[256,4]{0,1:T(4,128)}, ...), branch_computations={%region_0.0_spmd, %region_1.4_spmd} | conditional | flops 2230320384 | bytes 61874252 | solution.py:104
  124.7 2.5 fusion.8
  127.3 5.5 %fusion.3 = (f32[256,4]{0,1:T(4,128)S(1)}, f32[4096,256,4]{1,0,2:T(8,128)S(1)}) fusion(f32[4,4096]{1,0:T(4,128)S(1)} %get-tuple-element.33, f32[256,4]{0,1:T(4,128)} %get-tuple-element.32, pred[256,4096]{0,1:T(8,128)(4,1)S(1)} %fusion.8, bf16[128,4096]{0,1:T(8,128)(2,1)} %get-tuple-element.30, bf16[256,512]{1,0:T(8,128)(2,1)} %get-tuple-element.40), kind=kOutput, calls=%fused_computation.7 | convolution fusion | flops 1094712320 | bytes 19210240 | tf_op jit(solution)/shard_map/cond/branch_1_fun/qagd,adk->qagk/dot_general | solution.py:82
  132.8 6.8 %fusion.9 = f32[256,1,4,128]{3,0,2,1:T(8,128)S(1)} fusion(f32[4096,256,4]{1,0,2:T(8,128)S(1)} %get-tuple-element.44, f32[256,4]{0,1:T(4,128)S(1)} %broadcast_maximum_fusion, f32[4,4096]{1,0:T(4,128)S(1)} %get-tuple-element.33, f32[256,4]{0,1:T(4,128)S(1)} %copy-done.5, pred[256,4096]{0,1:T(8,128)(4,1)S(1)} %fusion.8, bf16[128,4096]{1,0:T(8,128)(2,1)S(1)} %copy-done.9), kind=kOutput, calls=%fused_computation.13 | convolution fusion | flops 1103101952 | bytes 19472384 | tf_op jit(solution)/shard_map/cond/branch_1_fun/qagk,adk->qagd/dot_general | solution.py:95
  139.7 5.8 %fusion.2 = f32[256,4]{0,1:T(4,128)S(1)} fusion(f32[4096,256,4]{1,0,2:T(8,128)S(1)} %get-tuple-element.44, f32[256,4]{0,1:T(4,128)S(1)} %broadcast_maximum_fusion, f32[4,4096]{1,0:T(4,128)S(1)} %get-tuple-element.33, f32[256,4]{0,1:T(4,128)S(1)} %copy-done.5, pred[256,4096]{0,1:T(8,128)(4,1)S(1)} %fusion.8), kind=kLoop, calls=%fused_computation.6 | loop fusion | flops 29359104 | bytes 17903616 | tf_op jit(solution)/shard_map/cond/branch_1_fun/reduce_sum | solution.py:94
  145.5 0.2 divide_convert_fusion
  145.7 0.2 copy.57
  146.0 3.9 %all_to_all.29 = bf16[2,128,512]{2,1,0:T(8,128)(2,1)S(1)} all-to-all(bf16[2,128,512]{2,1,0:T(8,128)(2,1)S(1)} %all_to_all.20), channel_id=1, replica_groups=mesh['sp'=16,'tp'=2] {'tp'}, dimensions={0} | all-to-all | bytes 524288 | tf_op jit(solution)/shard_map/all_to_all | solution.py:110
  149.9 0.2 copy.58
  150.1 2.9 convolution_convert_fusion.2
  153.1 0.3 fusion.40
  153.3 0.3 multiply_reduce_fusion.1
  153.7 0.3 multiply_convert_fusion.1
  154.0 1.2 convolution_convert_fusion.1
  155.2 96.7 %all_to_all.30 = bf16[32,32,2048]{2,1,0:T(8,128)(2,1)S(1)} all-to-all(bf16[32,32,2048]{2,1,0:T(8,128)(2,1)S(1)} %bitcast.161), channel_id=1, replica_groups=mesh['sp'=16,'tp'=2] {'sp','tp'}, dimensions={0} | all-to-all | bytes 8388608 | tf_op jit(solution)/shard_map/all_to_all | solution.py:132
  252.0 2.0 copy-done.3
  253.9 3.7 fusion.22
  257.7 10.1 %convolution_convert_fusion = bf16[32,32,2048]{2,1,0:T(8,128)(2,1)} fusion(bf16[1,512,2048]{2,1,0:T(8,128)(2,1)S(1)} %copy-done, f32[32,32,512]{2,1,0:T(8,128)} %fusion.22, bf16[32,32,2048]{2,1,0:T(8,128)(2,1)} %copy-done.3, bf16[1,2048,512]{2,1,0:T(8,128)(2,1)} %param.29), kind=kOutput, calls=%fused_computation.24 | convolution fusion | flops 4300210176 | bytes 14680064 | tf_op jit(solution)/shard_map/nemf,efd->nemd/dot_general | solution.py:29
  267.7 4.0 %all-to-all-start.2 = ((bf16[32,32,2048]{2,1,0:T(8,128)(2,1)}), bf16[32,32,2048]{2,1,0:T(8,128)(2,1)}, u32[]{:S(2)}, u32[]{:S(2)}) async-start(bf16[32,32,2048]{2,1,0:T(8,128)(2,1)} %convolution_convert_fusion), calls=%async_computation.2 | async-start | bytes 8388608 | tf_op jit(solution)/shard_map/all_to_all | solution.py:137
  271.8 0.1 copy.64
  271.9 0.1 mul.107
  272.0 0.1 copy.63
  272.2 0.2 copy.66
  272.4 2.0 fusion.58
  274.4 91.0 %all-to-all-done.2 = bf16[32,32,2048]{2,1,0:T(8,128)(2,1)} async-done(((bf16[32,32,2048]{2,1,0:T(8,128)(2,1)}), bf16[32,32,2048]{2,1,0:T(8,128)(2,1)}, u32[]{:S(2)}, u32[]{:S(2)}) %all-to-all-start.2) | async-done | bytes 4194336 | tf_op jit(solution)/shard_map/all_to_all | solution.py:137
  365.5 8.0 %gather_fusion = bf16[512,2048]{1,0:T(8,128)(2,1)} fusion(bf16[1024,2048]{1,0:T(8,128)(2,1)} %bitcast.35, s32[1024]{0:T(1024)S(1)} %pad_clamp_fusion), kind=kCustom, calls=%fused_computation | custom fusion | bytes 4196352 | tf_op jit(solution)/shard_map/jit(_take)/gather | solution.py:139
  373.5 4.1 %gather.7 = bf16[128,4,2048]{2,1,0:T(4,128)(2,1)} reshape(bf16[512,2048]{1,0:T(8,128)(2,1)} %gather_fusion) | data formatting | bytes 4194304 | tf_op jit(solution)/shard_map/jit(_take)/gather | solution.py:139
  377.6 3.9 fusion.29
  381.5 4.0 %fusion.57 = (f32[128]{0:T(128)S(1)}, f32[128,2048]{1,0:T(8,128)S(1)}) fusion(bf16[512,2048]{1,0:T(8,128)(2,1)} %param.34, bf16[128,2048]{1,0:T(8,128)(2,1)} %copy-done.1, bf16[2048,512]{1,0:T(8,128)(2,1)} %param.33, f32[128,512]{1,0:T(8,128)S(1)} %fusion.58, f32[128,1,2048]{2,1,0:T(1,128)} %fusion.29), kind=kOutput, calls=%fused_computation.85 | convolution fusion | flops 538574720 | bytes 7078400 | tf_op jit(solution)/shard_map/dot_general | solution.py:144
  385.5 0.3 multiply_reduce_fusion
  385.7 1.0 multiply_convert_fusion
  (40 shorter events, 0.4 us)
Async XLA Ops:
  6.5 251.1 %copy-start = (bf16[1,512,2048]{2,1,0:T(8,128)(2,1)S(1)}, bf16[1,512,2048]{2,1,0:T(8,128)(2,1)}, u32[]{:S(2)}) copy-start(bf16[1,512,2048]{2,1,0:T(8,128)(2,1)} %param.31) | copy-start | bytes 6291460
  6.5 88.9 %all-gather.5.cloned.1.call-start = ((), (), s32[]{:S(2)}) async-start(), calls=%async_computation.3 | async-start | bytes 1114112 | tf_op jit(solution)/shard_map/all_gather | solution.py:72
  8.3 116.4 %all-gather.7.cloned.1.call-start = ((), (), s32[]{:S(2)}) async-start(), calls=%async_computation.4 | async-start | bytes 1114112 | tf_op jit(solution)/shard_map/all_gather | solution.py:73
  127.3 5.5 %copy-start.5 = (f32[256,4]{0,1:T(4,128)S(1)}, f32[256,4]{0,1:T(4,128)}, u32[]{:S(2)}) copy-start(f32[256,4]{0,1:T(4,128)} %get-tuple-element.32) | copy-start | bytes 12292 | tf_op jit(solution)/shard_map/cond
  127.3 5.5 %copy-start.9 = (bf16[128,4096]{1,0:T(8,128)(2,1)S(1)}, bf16[128,4096]{1,0:T(8,128)(2,1)}, u32[]{:S(2)}) copy-start(bf16[128,4096]{1,0:T(8,128)(2,1)} %get-tuple-element.34) | copy-start | bytes 3145732 | tf_op jit(solution)/shard_map/cond
  145.5 7.6 %copy-start.2 = (bf16[128,2048]{1,0:T(8,128)(2,1)S(1)}, bf16[128,2048]{1,0:T(8,128)(2,1)}, u32[]{:S(2)}) copy-start(bf16[128,2048]{1,0:T(8,128)(2,1)} %param.24) | copy-start | bytes 1572868
  154.0 118.4 %copy-start.1 = (bf16[128,2048]{1,0:T(8,128)(2,1)}, bf16[128,2048]{1,0:T(8,128)(2,1)S(1)}, u32[]{:S(2)}) copy-start(bf16[128,2048]{1,0:T(8,128)(2,1)S(1)} %multiply_convert_fusion.1) | copy-start | bytes 1572868
  155.2 98.7 %copy-start.8 = (bf16[1,2048,512]{2,1,0:T(8,128)(2,1)S(1)}, bf16[1,2048,512]{2,1,0:T(8,128)(2,1)}, u32[]{:S(2)}) copy-start(bf16[1,2048,512]{2,1,0:T(8,128)(2,1)} %param.30) | copy-start | bytes 6291460
  252.0 2.0 copy-start.3
  267.7 4.0 %copy-start.4 = (s32[128,4]{0,1:T(4,128)S(1)}, s32[128,4]{0,1:T(4,128)}, u32[]{:S(2)}) copy-start(s32[128,4]{0,1:T(4,128)} %param.27) | copy-start | bytes 6148
  267.7 4.4 %copy-start.7 = (f32[128,4]{0,1:T(4,128)S(1)}, f32[128,4]{0,1:T(4,128)}, u32[]{:S(2)}) copy-start(f32[128,4]{0,1:T(4,128)} %param.28) | copy-start | bytes 6148
  267.7 4.6 %copy-start.6 = (bf16[2048]{0:T(1024)(128)(2,1)S(1)}, bf16[2048]{0:T(1024)(128)(2,1)}, u32[]{:S(2)}) copy-start(bf16[2048]{0:T(1024)(128)(2,1)} %param.35) | copy-start | bytes 12292
  267.7 97.7 %all-to-all-start.2 = ((bf16[32,32,2048]{2,1,0:T(8,128)(2,1)}), bf16[32,32,2048]{2,1,0:T(8,128)(2,1)}, u32[]{:S(2)}, u32[]{:S(2)}) async-start(bf16[32,32,2048]{2,1,0:T(8,128)(2,1)} %convolution_convert_fusion), calls=%async_computation.2 | async-start | bytes 8388608 | tf_op jit(solution)/shard_map/all_to_all | solution.py:137
Sparse Core Ops, SparseCore 0:
  10.1 57.9 all-gather.4
  70.8 53.9 all-gather.6
where the time goes:
time: 394 us
  blocking collectives  180 us (46%)
  waiting for transfers between devices  121 us (31%)
  matrix products  40.2 us (10%)
  local copies, waits for them, and re-layouts  20.1 us (5%)
  between operations  14.9 us (4%)
  other arithmetic  13.8 us (4%)
  starting transfers between devices  4.06 us (1%)
    all_to_all x1, blocking collectives, local(): lax.all_to_all(outgoing, ('sp', 'tp'), split_axis=0, concat_axis=0, tiled...  96.7 us
    all_to_all x1, waiting for transfers between devices, local(): lax.all_to_all(finished, ('sp', 'tp'), split_axis=0, concat_axis=0, tiled...  91 us
    all_gather x1, blocking collectives, local(): lax.all_gather(documents.reshape(1, tok_rows), 'sp', axis=1, tiled=True)  42.7 us
    all_gather x1, blocking collectives, local(): lax.all_gather(gate_cache, 'sp', axis=1, tiled=True)  36.1 us
    all_gather x1, waiting for transfers between devices, local(): value_piece = lax.all_gather(values, 'sp', axis=1, tiled=True)  29.3 us
    gather x2, local copies, waits for them, and re-layouts, local(): jnp.take(returned, slots, axis=0).reshape(row_count, top_count, width_model)  12.1 us
    dot_general x1, matrix products, expert_block(): jnp.einsum('nemf,efd->nemd', hidden, expert_down, preferred_element_type=...  10.1 us
  transfers between devices with their start and end apart: 3, of which 2 were waited for; matrix products, arithmetic and copies ran while one was open for 2% of the time, Pallas kernels for 0%

commit v1 on v0

--- a/solution.py
+++ b/solution.py
@@ -61,7 +61,7 @@
     grouped_q = queries.reshape(tok_rows, kv_local, group_size, HD)
     all_cache, all_docs = (
         lax.all_gather(gate_cache, "sp", axis=1, tiled=True),
-        lax.all_gather(documents.reshape(1, tok_rows), "sp", axis=1, tiled=True),
+        jnp.concatenate(lax.all_gather(documents.reshape(1, tok_rows), "sp"), axis=1),
     )
     doc_line = all_docs[0]
     initial = (

time: 394 us -> 394 us (level)
  no operation moved by 1% of the time
where the time goes in v1:
time: 394 us
  blocking collectives  180 us (46%)
  waiting for transfers between devices  121 us (31%)
  matrix products  40.2 us (10%)
  local copies, waits for them, and re-layouts  20.1 us (5%)
  between operations  14.9 us (4%)
  other arithmetic  13.8 us (4%)
  starting transfers between devices  4.06 us (1%)
    all_to_all x1, blocking collectives, local(): lax.all_to_all(outgoing, ('sp', 'tp'), split_axis=0, concat_axis=0, tiled...  96.7 us
    all_to_all x1, waiting for transfers between devices, local(): lax.all_to_all(finished, ('sp', 'tp'), split_axis=0, concat_axis=0, tiled...  91 us
    all_gather x1, blocking collectives, local(): lax.all_gather(documents.reshape(1, tok_rows), 'sp')  42.7 us
    all_gather x1, blocking collectives, local(): lax.all_gather(gate_cache, 'sp', axis=1, tiled=True)  36.1 us
    all_gather x1, waiting for transfers between devices, local(): value_piece = lax.all_gather(values, 'sp', axis=1, tiled=True)  29.3 us
    gather x2, local copies, waits for them, and re-layouts, local(): jnp.take(returned, slots, axis=0).reshape(row_count, top_count, width_model)  12.1 us
    dot_general x1, matrix products, expert_block(): jnp.einsum('nemf,efd->nemd', hidden, expert_down, preferred_element_type=...  10.1 us
  transfers between devices with their start and end apart: 3, of which 2 were waited for; matrix products, arithmetic and copies ran while one was open for 2% of the time, Pallas kernels for 0%

profile of v1, /device:TPU:0, one launch (start us, length us, event | category | flops | bytes accessed | tf_op | source)
XLA Modules:
  0.0 393.6 jit_solution(11862828123948388380)
XLA Ops:
  6.5 1.7 copy.56
  8.3 0.7 all-gather.7.cloned.1.call-update
  9.0 0.8 copy.59
  9.8 0.1 eq.59
  9.9 0.1 reshape.231
  10.1 1.2 slice.13
  11.3 42.7 %all-gather.1 = s32[16,1,256]{2,1,0:T(1,128)S(1)} all-gather(s32[1,1,256]{2,1,0:T(1,128)} %bitcast.170), channel_id=2, replica_groups=mesh['sp'=16,'tp'=2] {'sp'}, dimensions={0}, use_global_device_ids=true | all-gather | bytes 17408 | tf_op jit(solution)/shard_map/all_gather | solution.py:64
  54.0 0.6 slice.19
  55.8 0.7 convert_element_type.60
  56.5 1.2 reduce-window.6
  57.7 0.2 slice_reduce_fusion
  58.0 0.1 fusion.50
  58.1 0.1 sub.47
  58.3 36.1 %all_gather.14 = f32[4,4096]{1,0:T(4,128)S(1)} all-gather(f32[4,256]{1,0:T(4,128)} %param.22), channel_id=1, replica_groups=mesh['sp'=16,'tp'=2] {'sp'}, dimensions={1}, use_global_device_ids=true | all-gather | bytes 69632 | tf_op jit(solution)/shard_map/all_gather | solution.py:63
  94.4 0.7 compare_and_fusion
  95.1 0.4 fusion.31
  95.4 29.3 %all-gather.7.cloned.1.call-done = bf16[128,4096]{1,0:T(8,128)(2,1)} async-done(((bf16[128,256]{1,0:T(8,128)(2,1)}), bf16[128,4096]{1,0:T(8,128)(2,1)}) %all-gather.7.cloned.1.call-update) | async-done | bytes 1048592 | tf_op jit(solution)/shard_map/all_gather | solution.py:73
  124.7 20.7 %conditional.1 = (f32[256,1,4]{0,2,1:T(4,128)S(1)}, f32[256,1,4,128]{3,0,2,1:T(8,128)S(1)}) conditional(s32[]{:T(128)} %convert_element_type.56, () %tuple.13, (s32[]{:T(128)}, s32[256]{0:T(256)S(1)}, s32[16,1,256]{2,1,0:T(1,128)S(1)}, s32[256]{0:T(256)}, bf16[256,512]{1,0:T(8,128)(2,1)}, /*index=5*/bf16[128,4096]{0,1:T(8,128)(2,1)}, ...), branch_computations={%region_0.0_spmd, %region_1.4_spmd} | conditional | flops 2230320384 | bytes 61874252 | solution.py:104
  124.7 2.5 fusion.8
  127.3 5.5 %fusion.3 = (f32[256,4]{0,1:T(4,128)S(1)}, f32[4096,256,4]{1,0,2:T(8,128)S(1)}) fusion(f32[4,4096]{1,0:T(4,128)S(1)} %get-tuple-element.33, f32[256,4]{0,1:T(4,128)} %get-tuple-element.32, pred[256,4096]{0,1:T(8,128)(4,1)S(1)} %fusion.8, bf16[128,4096]{0,1:T(8,128)(2,1)} %get-tuple-element.30, bf16[256,512]{1,0:T(8,128)(2,1)} %get-tuple-element.40), kind=kOutput, calls=%fused_computation.7 | convolution fusion | flops 1094712320 | bytes 19210240 | tf_op jit(solution)/shard_map/cond/branch_1_fun/qagd,adk->qagk/dot_general | solution.py:82
  132.8 6.8 %fusion.9 = f32[256,1,4,128]{3,0,2,1:T(8,128)S(1)} fusion(f32[4096,256,4]{1,0,2:T(8,128)S(1)} %get-tuple-element.44, f32[256,4]{0,1:T(4,128)S(1)} %broadcast_maximum_fusion, f32[4,4096]{1,0:T(4,128)S(1)} %get-tuple-element.33, f32[256,4]{0,1:T(4,128)S(1)} %copy-done.5, pred[256,4096]{0,1:T(8,128)(4,1)S(1)} %fusion.8, bf16[128,4096]{1,0:T(8,128)(2,1)S(1)} %copy-done.9), kind=kOutput, calls=%fused_computation.13 | convolution fusion | flops 1103101952 | bytes 19472384 | tf_op jit(solution)/shard_map/cond/branch_1_fun/qagk,adk->qagd/dot_general | solution.py:95
  139.7 5.8 %fusion.2 = f32[256,4]{0,1:T(4,128)S(1)} fusion(f32[4096,256,4]{1,0,2:T(8,128)S(1)} %get-tuple-element.44, f32[256,4]{0,1:T(4,128)S(1)} %broadcast_maximum_fusion, f32[4,4096]{1,0:T(4,128)S(1)} %get-tuple-element.33, f32[256,4]{0,1:T(4,128)S(1)} %copy-done.5, pred[256,4096]{0,1:T(8,128)(4,1)S(1)} %fusion.8), kind=kLoop, calls=%fused_computation.6 | loop fusion | flops 29359104 | bytes 17903616 | tf_op jit(solution)/shard_map/cond/branch_1_fun/reduce_sum | solution.py:94
  145.5 0.2 divide_convert_fusion
  145.7 0.2 copy.57
  146.0 3.9 %all_to_all.29 = bf16[2,128,512]{2,1,0:T(8,128)(2,1)S(1)} all-to-all(bf16[2,128,512]{2,1,0:T(8,128)(2,1)S(1)} %all_to_all.20), channel_id=1, replica_groups=mesh['sp'=16,'tp'=2] {'tp'}, dimensions={0} | all-to-all | bytes 524288 | tf_op jit(solution)/shard_map/all_to_all | solution.py:110
  149.9 0.2 copy.58
  150.1 2.9 convolution_convert_fusion.2
  153.1 0.3 fusion.40
  153.3 0.3 multiply_reduce_fusion.1
  153.7 0.3 multiply_convert_fusion.1
  154.0 1.2 convolution_convert_fusion.1
  155.2 96.7 %all_to_all.30 = bf16[32,32,2048]{2,1,0:T(8,128)(2,1)S(1)} all-to-all(bf16[32,32,2048]{2,1,0:T(8,128)(2,1)S(1)} %bitcast.160), channel_id=1, replica_groups=mesh['sp'=16,'tp'=2] {'sp','tp'}, dimensions={0} | all-to-all | bytes 8388608 | tf_op jit(solution)/shard_map/all_to_all | solution.py:132
  252.0 2.0 copy-done.3
  253.9 3.7 fusion.22
  257.7 10.1 %convolution_convert_fusion = bf16[32,32,2048]{2,1,0:T(8,128)(2,1)} fusion(bf16[1,512,2048]{2,1,0:T(8,128)(2,1)S(1)} %copy-done, f32[32,32,512]{2,1,0:T(8,128)} %fusion.22, bf16[32,32,2048]{2,1,0:T(8,128)(2,1)} %copy-done.3, bf16[1,2048,512]{2,1,0:T(8,128)(2,1)} %param.29), kind=kOutput, calls=%fused_computation.24 | convolution fusion | flops 4300210176 | bytes 14680064 | tf_op jit(solution)/shard_map/nemf,efd->nemd/dot_general | solution.py:29
  267.7 4.0 %all-to-all-start.2 = ((bf16[32,32,2048]{2,1,0:T(8,128)(2,1)}), bf16[32,32,2048]{2,1,0:T(8,128)(2,1)}, u32[]{:S(2)}, u32[]{:S(2)}) async-start(bf16[32,32,2048]{2,1,0:T(8,128)(2,1)} %convolution_convert_fusion), calls=%async_computation.2 | async-start | bytes 8388608 | tf_op jit(solution)/shard_map/all_to_all | solution.py:137
  271.8 0.1 copy.64
  271.9 0.1 mul.107
  272.0 0.1 copy.63
  272.2 0.2 copy.66
  272.4 2.0 fusion.58
  274.4 91.0 %all-to-all-done.2 = bf16[32,32,2048]{2,1,0:T(8,128)(2,1)} async-done(((bf16[32,32,2048]{2,1,0:T(8,128)(2,1)}), bf16[32,32,2048]{2,1,0:T(8,128)(2,1)}, u32[]{:S(2)}, u32[]{:S(2)}) %all-to-all-start.2) | async-done | bytes 4194336 | tf_op jit(solution)/shard_map/all_to_all | solution.py:137
  365.5 8.0 %gather_fusion = bf16[512,2048]{1,0:T(8,128)(2,1)} fusion(bf16[1024,2048]{1,0:T(8,128)(2,1)} %bitcast.34, s32[1024]{0:T(1024)S(1)} %pad_clamp_fusion), kind=kCustom, calls=%fused_computation | custom fusion | bytes 4196352 | tf_op jit(solution)/shard_map/jit(_take)/gather | solution.py:139
  373.5 4.1 %gather.7 = bf16[128,4,2048]{2,1,0:T(4,128)(2,1)} reshape(bf16[512,2048]{1,0:T(8,128)(2,1)} %gather_fusion) | data formatting | bytes 4194304 | tf_op jit(solution)/shard_map/jit(_take)/gather | solution.py:139
  377.6 3.9 fusion.29
  381.5 4.0 %fusion.57 = (f32[128]{0:T(128)S(1)}, f32[128,2048]{1,0:T(8,128)S(1)}) fusion(bf16[512,2048]{1,0:T(8,128)(2,1)} %param.34, bf16[128,2048]{1,0:T(8,128)(2,1)} %copy-done.1, bf16[2048,512]{1,0:T(8,128)(2,1)} %param.33, f32[128,512]{1,0:T(8,128)S(1)} %fusion.58, f32[128,1,2048]{2,1,0:T(1,128)} %fusion.29), kind=kOutput, calls=%fused_computation.85 | convolution fusion | flops 538574720 | bytes 7078400 | tf_op jit(solution)/shard_map/dot_general | solution.py:144
  385.5 0.3 multiply_reduce_fusion
  385.7 1.0 multiply_convert_fusion
  (40 shorter events, 0.4 us)
Async XLA Ops:
  6.5 251.1 %copy-start = (bf16[1,512,2048]{2,1,0:T(8,128)(2,1)S(1)}, bf16[1,512,2048]{2,1,0:T(8,128)(2,1)}, u32[]{:S(2)}) copy-start(bf16[1,512,2048]{2,1,0:T(8,128)(2,1)} %param.31) | copy-start | bytes 6291460
  6.5 88.9 %all-gather.5.cloned.1.call-start = ((), (), s32[]{:S(2)}) async-start(), calls=%async_computation.3 | async-start | bytes 1114112 | tf_op jit(solution)/shard_map/all_gather | solution.py:72
  8.3 116.4 %all-gather.7.cloned.1.call-start = ((), (), s32[]{:S(2)}) async-start(), calls=%async_computation.4 | async-start | bytes 1114112 | tf_op jit(solution)/shard_map/all_gather | solution.py:73
  127.3 5.5 %copy-start.5 = (f32[256,4]{0,1:T(4,128)S(1)}, f32[256,4]{0,1:T(4,128)}, u32[]{:S(2)}) copy-start(f32[256,4]{0,1:T(4,128)} %get-tuple-element.32) | copy-start | bytes 12292 | tf_op jit(solution)/shard_map/cond
  127.3 5.5 %copy-start.9 = (bf16[128,4096]{1,0:T(8,128)(2,1)S(1)}, bf16[128,4096]{1,0:T(8,128)(2,1)}, u32[]{:S(2)}) copy-start(bf16[128,4096]{1,0:T(8,128)(2,1)} %get-tuple-element.34) | copy-start | bytes 3145732 | tf_op jit(solution)/shard_map/cond
  145.5 7.6 %copy-start.2 = (bf16[128,2048]{1,0:T(8,128)(2,1)S(1)}, bf16[128,2048]{1,0:T(8,128)(2,1)}, u32[]{:S(2)}) copy-start(bf16[128,2048]{1,0:T(8,128)(2,1)} %param.24) | copy-start | bytes 1572868
  154.0 118.4 %copy-start.1 = (bf16[128,2048]{1,0:T(8,128)(2,1)}, bf16[128,2048]{1,0:T(8,128)(2,1)S(1)}, u32[]{:S(2)}) copy-start(bf16[128,2048]{1,0:T(8,128)(2,1)S(1)} %multiply_convert_fusion.1) | copy-start | bytes 1572868
  155.2 98.7 %copy-start.8 = (bf16[1,2048,512]{2,1,0:T(8,128)(2,1)S(1)}, bf16[1,2048,512]{2,1,0:T(8,128)(2,1)}, u32[]{:S(2)}) copy-start(bf16[1,2048,512]{2,1,0:T(8,128)(2,1)} %param.30) | copy-start | bytes 6291460
  252.0 2.0 copy-start.3
  267.7 4.0 %copy-start.4 = (s32[128,4]{0,1:T(4,128)S(1)}, s32[128,4]{0,1:T(4,128)}, u32[]{:S(2)}) copy-start(s32[128,4]{0,1:T(4,128)} %param.27) | copy-start | bytes 6148
  267.7 4.4 %copy-start.7 = (f32[128,4]{0,1:T(4,128)S(1)}, f32[128,4]{0,1:T(4,128)}, u32[]{:S(2)}) copy-start(f32[128,4]{0,1:T(4,128)} %param.28) | copy-start | bytes 6148
  267.7 4.6 %copy-start.6 = (bf16[2048]{0:T(1024)(128)(2,1)S(1)}, bf16[2048]{0:T(1024)(128)(2,1)}, u32[]{:S(2)}) copy-start(bf16[2048]{0:T(1024)(128)(2,1)} %param.35) | copy-start | bytes 12292
  267.7 97.7 %all-to-all-start.2 = ((bf16[32,32,2048]{2,1,0:T(8,128)(2,1)}), bf16[32,32,2048]{2,1,0:T(8,128)(2,1)}, u32[]{:S(2)}, u32[]{:S(2)}) async-start(bf16[32,32,2048]{2,1,0:T(8,128)(2,1)} %convolution_convert_fusion), calls=%async_computation.2 | async-start | bytes 8388608 | tf_op jit(solution)/shard_map/all_to_all | solution.py:137
Sparse Core Ops, SparseCore 0:
  10.1 57.9 all-gather.4
  70.8 53.9 all-gather.6
